TPU v7x, 256 devices: a whole 4x4x8 slice. The times are simulated.
256 devices in a mesh: sp: 64 (over z, y, core), tp: 4 (over x).
Axes of the slice: x: 4, y: 4, z: 8, core: 2. Of those that a mesh axis runs over, the one named last changes fastest.
Arguments:
- stream_in: bfloat16 [49152, 2048], P(('sp', 'tp')), may hold values from -6 to 6
- query_wide: bfloat16 [49152, 512], P('sp', 'tp'), may hold values from -6 to 6
- key_wide: bfloat16 [49152, 512], P('sp', 'tp'), may hold values from -6 to 6
- value_wide: bfloat16 [49152, 512], P('sp', 'tp'), may hold values from -6 to 6
- gate_wide: bfloat16 [49152, 512], P('sp', 'tp'), may hold values from -6 to 6
- decay_wide: float32 [4, 49152], P('tp', 'sp'), may hold values from -2.3 to 0, as said below
- query_narrow: bfloat16 [49152, 512], P('sp', 'tp'), may hold values from -6 to 6
- key_narrow: bfloat16 [49152, 512], P('sp', 'tp'), may hold values from -6 to 6
- value_narrow: bfloat16 [49152, 512], P('sp', 'tp'), may hold values from -6 to 6
- gate_narrow: bfloat16 [49152, 512], P('sp', 'tp'), may hold values from -6 to 6
- decay_narrow: float32 [8, 49152], P('tp', 'sp'), may hold values from -2.3 to 0, as said below
- output_wide: bfloat16 [512, 2048], P('tp'), may hold values from -0.25 to 0.25
- output_narrow: bfloat16 [512, 2048], P('tp'), may hold values from -0.25 to 0.25
- norm_gain: bfloat16 [2048], replicated, may hold values from 0.099609375 to 1.8984375
- up_weight: bfloat16 [2048, 8192], P('sp', 'tp'), may hold values from -0.125 to 0.125
- down_weight: bfloat16 [8192, 2048], P('tp', 'sp'), may hold values from -0.0625 to 0.0625
Outputs:
- layer_out: bfloat16 [49152, 2048], P(('sp', 'tp'))
Inputs may be any that keep to these rules, and one draw needn't show every extreme that they name: `decay_wide`: each entry is the logarithm of one head's retention factor at one position. `decay_narrow`: each entry is the logarithm of one head's retention factor at one position.
All inputs are finite; a program needn't handle non-finite values.
Results may differ from a plain program's by a relative error of at most 0.02.
Values may be sent and summed in bfloat16 or wider, within the bound.
A program may use at most 128 MiB of HBM per device.

v0:
```python
import jax
import jax.numpy as jnp
from jax import lax
from jax.sharding import Mesh
from jax.sharding import PartitionSpec as P

HDW = 128
HDN = 64
BLOCK = 128
SP = ("sp_0", "sp_1", "sp_2")
SP_TP = ("sp_0", "sp_1", "sp_2", "tp")
head_eps = 1e-05
norm_eps = 1e-06
rope_base = 10000.0


def rows_first(arrays, axis, dims):
    turned = [jnp.moveaxis(a, dim, 0) for a, dim in zip(arrays, dims)]
    both = jnp.concatenate([t.reshape(len(t), -1) for t in turned], axis=1)
    out, at, finished = (lax.all_gather(both, axis, axis=0, tiled=True), 0, [])
    for t, dim in zip(turned, dims):
        section = out[:, at : at + t[0].size].reshape(-1, *t.shape[1:])
        finished.append(jnp.moveaxis(section, 0, dim))
        at += t[0].size
    return tuple(finished)


def nothing_yet(shard, identity):
    return jax.tree.map(
        lambda part, zero: jnp.zeros_like(part) + jnp.asarray(zero, part.dtype), shard, identity
    )


def gathered_once(shard, axis):
    leaves = jax.tree.leaves(shard)
    sequence = sorted(range(len(leaves)), key=lambda k: -leaves[k].size)
    width = (1, *leaves[sequence[0]].shape)[-1]
    lines = [
        jnp.pad(leaves[k].reshape(-1), (0, -leaves[k].size % width)).reshape(-1, width)
        for k in sequence
    ]
    both, at, found = (lax.all_gather(jnp.concatenate(lines), axis), 0, {})
    for k, line in zip(sequence, lines):
        section = both[:, at : at + len(line)].reshape(len(both), -1)
        found[k] = section[:, : leaves[k].size].reshape(-1, *leaves[k].shape)
        at += len(line)
    numbers = iter(range(len(leaves)))
    return jax.tree.map(lambda _: found[next(numbers)], shard)


def entering(shard, axes, combine, identity):
    before = start = nothing_yet(shard, identity)
    so_far = shard
    for axis in reversed(axes):
        length, mine = (lax.axis_size(axis), lax.axis_index(axis))
        pieces = gathered_once(
            jax.tree.map(
                lambda part, kind: part.astype(kind),
                so_far,
                (jnp.bfloat16, jnp.bfloat16, jnp.bfloat16, jnp.bfloat16),
            ),
            axis,
        )
        inside, so_far = (start, start)
        for k in range(length):
            passed = k < mine
            so_far = combine(
                so_far, jax.tree.map(lambda part, own: part[k].astype(own.dtype), pieces, shard)
            )
            inside = jax.tree.map(lambda new, old: jnp.where(passed, new, old), so_far, inside)
        before = combine(inside, before)
    return before


def in_blocks(shard, dim, length):
    before, after = (shard.shape[:dim], shard.shape[dim + 1 :])
    return jnp.moveaxis(shard.reshape(*before, length, -1, *after), dim, 0)


def sum_at_owner(shard, axis, dim):
    tiles = in_blocks(shard, dim, lax.axis_size(axis))
    arrived = lax.all_to_all(tiles, axis, split_axis=0, concat_axis=0, tiled=True)
    return arrived.astype(jnp.float32).sum(axis=0)


def rotate(values, places):
    half = values.shape[-1] // 2
    inverse = rope_base ** (-jnp.arange(half, dtype=jnp.float32) / half)
    angles = places[:, None] * inverse[None, :]
    cosine = jnp.cos(angles)[:, None, :]
    sine = jnp.sin(angles)[:, None, :]
    front = values[..., :half]
    back = values[..., half:]
    return jnp.concatenate([front * cosine - back * sine, back * cosine + front * sine], axis=-1)


def block_step(carried, inputs):
    query, keys, values, log_rate = inputs
    running = jnp.cumsum(log_rate, axis=0)
    spread = running[:, None, :] - running[None, :, :]
    length = log_rate.shape[0]
    lower = (jnp.arange(length)[:, None] >= jnp.arange(length)[None, :])[:, :, None]
    factor = jnp.where(lower, jnp.exp(jnp.minimum(spread, 0.0)), 0.0)
    scores = jnp.einsum("thd,shd->tsh", query, keys) * factor
    within = jnp.einsum("tsh,she->the", scores, values)
    across = jnp.einsum("thd,hde->the", query, carried) * jnp.exp(running)[:, :, None]
    tail_decay = jnp.exp(running[-1][None, :] - running)
    updated = jnp.exp(running[-1])[:, None, None] * carried + jnp.einsum(
        "shd,she->hde", keys * tail_decay[:, :, None], values
    )
    return (updated, within + across)


def head_norm(values):
    centre = values - jnp.mean(values, axis=-1, keepdims=True)
    spread = jnp.mean(centre * centre, axis=-1, keepdims=True)
    return centre * lax.rsqrt(spread + head_eps)


def local_group(query, keys, values, log_rate, width, places):
    length = query.shape[0]
    count_of_heads = query.shape[1] // width
    blocks = length // BLOCK

    def split(array):
        return array.astype(jnp.float32).reshape(length, count_of_heads, width)

    query_rot = rotate(split(query), places)
    keys_rot = rotate(split(keys), places) * width ** (-0.5)
    rates = log_rate.T
    carried = jnp.zeros((count_of_heads, width, width), jnp.float32)
    final_state, outputs = lax.scan(
        block_step,
        carried,
        (
            query_rot.reshape(blocks, BLOCK, count_of_heads, width),
            keys_rot.reshape(blocks, BLOCK, count_of_heads, width),
            split(values).reshape(blocks, BLOCK, count_of_heads, width),
            rates.reshape(blocks, BLOCK, count_of_heads),
        ),
    )
    running = jnp.cumsum(rates, axis=0)
    return (
        query_rot,
        outputs.reshape(length, count_of_heads, width),
        final_state,
        jnp.exp(running[-1]),
        running,
    )


def finish_group(query_rot, outputs, incoming, running, gate):
    length = outputs.shape[0]
    outputs = (
        outputs + jnp.einsum("thd,hde->the", query_rot, incoming) * jnp.exp(running)[:, :, None]
    )
    normed = head_norm(outputs).reshape(length, -1)
    return (jax.nn.silu(gate.astype(jnp.float32)) * normed).astype(jnp.bfloat16)


def chain(earlier, later):
    rate_wide, memory_wide, rate_narrow, memory_narrow = earlier
    later_rate_wide, later_memory_wide, later_rate_narrow, later_memory_narrow = later
    return (
        rate_wide * later_rate_wide,
        memory_wide * later_rate_wide[:, None, None] + later_memory_wide,
        rate_narrow * later_rate_narrow,
        memory_narrow * later_rate_narrow[:, None, None] + later_memory_narrow,
    )


def row_norm(middle, norm_gain):
    middle_f = middle.astype(jnp.float32)
    scale = lax.rsqrt(jnp.mean(middle_f * middle_f, axis=-1, keepdims=True) + norm_eps)
    return (middle_f * scale * norm_gain.astype(jnp.float32)).astype(jnp.bfloat16)


def on_device(
    stream_in,
    query_wide,
    key_wide,
    value_wide,
    gate_wide,
    decay_wide,
    query_narrow,
    key_narrow,
    value_narrow,
    gate_narrow,
    decay_narrow,
    output_wide,
    output_narrow,
    norm_gain,
    up_weight,
    down_weight,
):
    length = query_wide.shape[0]
    up_full, down_full = rows_first((up_weight, down_weight), SP, (0, 1))
    places = (lax.axis_index(SP) * length + jnp.arange(length, dtype=jnp.int32)).astype(jnp.float32)
    wide_query, wide_out, wide_state, wide_total, wide_running = local_group(
        query_wide, key_wide, value_wide, decay_wide, HDW, places
    )
    narrow_query, narrow_out, narrow_state, narrow_total, narrow_running = local_group(
        query_narrow, key_narrow, value_narrow, decay_narrow, HDN, places
    )
    identity = (
        jnp.ones_like(wide_total),
        jnp.zeros_like(wide_state),
        jnp.ones_like(narrow_total),
        jnp.zeros_like(narrow_state),
    )
    incoming = entering((wide_total, wide_state, narrow_total, narrow_state), SP, chain, identity)
    mixed_wide = finish_group(wide_query, wide_out, incoming[1], wide_running, gate_wide)
    mixed_narrow = finish_group(narrow_query, narrow_out, incoming[3], narrow_running, gate_narrow)
    mixed_sum = sum_at_owner(
        (
            jnp.dot(mixed_wide, output_wide, preferred_element_type=jnp.float32)
            + jnp.dot(mixed_narrow, output_narrow, preferred_element_type=jnp.float32)
        ).astype(jnp.bfloat16),
        "tp",
        0,
    )
    middle = (stream_in.astype(jnp.float32) + mixed_sum).astype(jnp.bfloat16)
    normed = lax.all_gather(row_norm(middle, norm_gain), "tp", axis=0, tiled=True)
    up_sum = jnp.dot(normed, up_full, preferred_element_type=jnp.float32)
    hidden = jnp.square(jax.nn.relu(up_sum)).astype(jnp.bfloat16)
    down_sum = jnp.dot(hidden, down_full, preferred_element_type=jnp.float32)
    down_rows = lax.psum_scatter(
        down_sum.astype(jnp.bfloat16), "tp", scatter_dimension=0, tiled=True
    ).astype(jnp.float32)
    return (middle.astype(jnp.float32) + down_rows).astype(jnp.bfloat16)


def solution(mesh):
    split = Mesh(mesh.devices.reshape(8, 4, 2, mesh.shape["tp"]), ("sp_0", "sp_1", "sp_2", "tp"))
    in_specs = (
        P(SP_TP, None),
        P(SP, "tp"),
        P(SP, "tp"),
        P(SP, "tp"),
        P(SP, "tp"),
        P("tp", SP),
        P(SP, "tp"),
        P(SP, "tp"),
        P(SP, "tp"),
        P(SP, "tp"),
        P("tp", SP),
        P("tp", None),
        P("tp", None),
        P(),
        P(SP, "tp"),
        P("tp", SP),
    )
    out_specs = P(SP_TP, None)
    return jax.shard_map(
        on_device, mesh=split, in_specs=in_specs, out_specs=out_specs, check_vma=False
    )
```

profile of v0, /device:TPU:1, one launch (start us, length us, event | category | flops | bytes accessed | tf_op | source)
XLA Modules:
  0.0 398.5 jit_solution(7533716243381743910)
XLA Ops:
  6.6 1.1 copy.156
  7.8 1.1 copy.158
  10.4 25.0 %while.27 = (s32[]{:T(128)}, f32[2,64,64]{2,1,0:T(8,128)S(1)}, f32[6,128,2,64]{1,0,3,2:T(8,128)}, f32[6,128,2]{2,1,0:T(8,128)S(1)}, f32[6,128,2,64]{1,0,3,2:T(8,...) while((s32[]{:T(128)}, f32[2,64,64]{2,1,0:T(8,128)S(1)}, ...), condition=%wide.region_5.6_spmd.clone, body=%wide.region_3.5_spmd.clone.sunk | while | flops 12877827 | bytes 1099440 | solution.py:132
  11.5 2.8 dynamic_update_slice.14
  15.7 2.8 dynamic_update_slice.14
  19.9 2.8 dynamic_update_slice.14
  24.0 2.8 dynamic_update_slice.14
  28.2 2.8 dynamic_update_slice.14
  32.3 2.8 dynamic_update_slice.14
  35.5 1.0 reshape_reshape.22
  36.5 1.9 fusion.88
  38.6 0.9 maximum_multiply_fusion.1
  39.5 22.9 %while.26 = (s32[]{:T(128)}, f32[1,128,128]{2,1,0:T(8,128)S(1)}, f32[6,128,1,128]{3,1,0,2:T(8,128)}, f32[6,128,1]{1,2,0:T(1,128)S(1)}, f32[6,128,1,128]{3,2,1,0:...) while((s32[]{:T(128)}, f32[1,128,128]{2,1,0:T(8,128)S(1)}, ...), condition=%wide.region_2.3_spmd.clone, body=%wide.region_0.2_spmd.clone.sunk | while | flops 17006596 | bytes 1515172 | solution.py:132
  40.5 0.6 fusion.342
  41.9 0.6 constant_dynamic-update-slice_fusion.2
  44.3 0.6 fusion.342
  45.7 0.6 constant_dynamic-update-slice_fusion.2
  49.6 0.6 constant_dynamic-update-slice_fusion.2
  53.4 0.6 constant_dynamic-update-slice_fusion.2
  57.2 0.6 constant_dynamic-update-slice_fusion.2
  61.0 0.6 constant_dynamic-update-slice_fusion.2
  63.2 0.6 slice.432
  63.8 0.7 slice.431
  65.8 0.6 reduce-window.14
  67.1 4.7 %all-gather.3 = bf16[2,194,128]{2,1,0:T(8,128)(2,1)S(1)} all-gather(bf16[1,194,128]{2,1,0:T(8,128)(2,1)S(1)} %maximum_bitcast_fusion), channel_id=2, replica_groups=mesh['sp_0'=8,'sp_1'=4,'sp_2'=2,'tp'=4] {'sp_2'}, dimensions={0}, use_global_device_ids=true | all-gather | bytes 148992 | tf_op jit(solution)/shard_map/all_gather | solution.py:42
  74.8 9.3 %all-gather.4 = bf16[4,194,128]{2,1,0:T(8,128)(2,1)S(1)} all-gather(bf16[1,194,128]{2,1,0:T(8,128)(2,1)S(1)} %maximum_bitcast_fusion.1), channel_id=3, replica_groups=mesh['sp_0'=8,'sp_1'=4,'sp_2'=2,'tp'=4] {'sp_1'}, dimensions={0}, use_global_device_ids=true | all-gather | bytes 248320 | tf_op jit(solution)/shard_map/all_gather | solution.py:42
  87.2 0.6 fusion.271
  89.2 21.5 %all-gather.5 = bf16[8,194,128]{2,1,0:T(8,128)(2,1)S(1)} all-gather(bf16[1,194,128]{2,1,0:T(8,128)(2,1)S(1)} %maximum_bitcast_fusion.2), channel_id=4, replica_groups=mesh['sp_0'=8,'sp_1'=4,'sp_2'=2,'tp'=4] {'sp_0'}, dimensions={0}, use_global_device_ids=true | all-gather | bytes 446976 | tf_op jit(solution)/shard_map/all_gather | solution.py:42
  110.7 0.6 bitcast_convert_fusion.8
  111.9 0.6 slice_convert_fusion.11
  112.5 0.7 fusion.269
  113.8 0.7 copy.176
  114.5 0.7 copy.177
  115.3 0.7 copy.178
  116.1 0.7 copy.179
  116.9 0.7 copy.180
  117.6 0.8 reshape.1118
  118.4 0.7 copy.181
  119.1 0.8 reshape.1119
  119.9 0.7 copy.182
  120.6 0.8 reshape.1120
  121.5 0.7 copy.183
  122.2 0.8 reshape.1121
  123.0 0.7 copy.184
  123.8 0.7 copy.185
  124.6 0.7 copy.186
  125.4 1.6 fusion.292
  127.1 1.1 copy.170
  128.2 0.6 fusion.288
  134.7 1.2 copy.169
  136.6 1.2 fusion.291
  137.8 1.1 copy.153
  139.1 1.0 fusion.93
  140.1 2.7 add_convert_fusion
  142.8 4.8 %all-to-all-start = ((bf16[4,192,2048]{2,1,0:T(8,128)(2,1)}), bf16[4,192,2048]{2,1,0:T(8,128)(2,1)}, u32[]{:S(2)}, u32[]{:S(2)}) async-start(bf16[4,192,2048]{2,1,0:T(8,128)(2,1)} %bitcast.454), calls=%async_computation | async-start | bytes 6291456 | tf_op jit(solution)/shard_map/all_to_all | solution.py:82
  147.8 27.9 %all-to-all-done = bf16[4,192,2048]{2,1,0:T(8,128)(2,1)} async-done(((bf16[4,192,2048]{2,1,0:T(8,128)(2,1)}), bf16[4,192,2048]{2,1,0:T(8,128)(2,1)}, u32[]{:S(2)}, u32[]{:S(2)}) %all-to-all-start) | async-done | bytes 3145760 | tf_op jit(solution)/shard_map/all_to_all | solution.py:82
  175.8 2.7 convert_reduce_fusion
  178.8 1.1 fusion.63
  180.1 0.7 pad_maximum_fusion.2
  180.9 47.7 %all-gather.9.cloned.1.call-done = bf16[768,2048]{1,0:T(8,128)(2,1)} async-done(((bf16[192,2048]{1,0:T(8,128)(2,1)}), bf16[768,2048]{1,0:T(8,128)(2,1)}) %all-gather.9.cloned.1.call-update) | async-done | bytes 3145744 | tf_op jit(solution)/shard_map/all_gather | solution.py:223
  228.6 102.9 %all-gather.11.cloned.1.call-done = bf16[2048,4096]{1,0:T(8,128)(2,1)} async-done(((bf16[32,4096]{1,0:T(8,128)(2,1)}), bf16[2048,4096]{1,0:T(8,128)(2,1)}) %all-gather.11.cloned.1.call-update) | async-done | bytes 16777232 | tf_op jit(solution)/shard_map/all_gather | solution.py:20
  331.5 20.7 %fusion.55 = bf16[768,2048]{1,0:T(8,128)(2,1)} fusion(bf16[2048,4096]{1,0:T(8,128)(2,1)} %all-gather.11.cloned.1.call-done, bf16[768,2048]{1,0:T(8,128)(2,1)} %all-gather.9.cloned.1.call-done), kind=kOutput, calls=%fused_computation.75 | convolution fusion | flops 12891193344 | bytes 23068672 | tf_op jit(solution)/shard_map/dot_general | solution.py:226
  352.2 37.5 %reduce-scatter.2.cloned.1.call-done = bf16[192,2048]{1,0:T(8,128)(2,1)} async-done(((bf16[768,2048]{1,0:T(8,128)(2,1)}), bf16[192,2048]{1,0:T(8,128)(2,1)}) %reduce-scatter.2.cloned.1.call-update) | async-done | bytes 786448 | tf_op jit(solution)/shard_map/reduce_scatter | solution.py:227
  389.7 2.3 fusion.64
  (288 shorter events, 29.7 us)
Async XLA Ops:
  6.5 132.5 %copy-start = (bf16[128,2048]{1,0:T(8,128)(2,1)S(1)}, bf16[128,2048]{1,0:T(8,128)(2,1)}, u32[]{:S(2)}) copy-start(bf16[128,2048]{1,0:T(8,128)(2,1)} %param.31) | copy-start | bytes 1572868
  6.5 3.0 copy-start.6
  7.8 2.3 copy-start.9
  10.4 26.1 %copy-start.4 = (bf16[768,128]{1,0:T(8,128)(2,1)S(1)}, bf16[768,128]{1,0:T(8,128)(2,1)}, u32[]{:S(2)}) copy-start(bf16[768,128]{1,0:T(8,128)(2,1)} %param.21) | copy-start | bytes 589828
  10.4 26.0 %copy-start.5 = (bf16[768,128]{1,0:T(8,128)(2,1)S(1)}, bf16[768,128]{1,0:T(8,128)(2,1)}, u32[]{:S(2)}) copy-start(bf16[768,128]{1,0:T(8,128)(2,1)} %param.22) | copy-start | bytes 589828
  36.5 3.0 copy-start.14
  71.8 15.4 %copy-start.15 = (f32[2]{0:T(128)}, f32[2]{0:T(128)S(1)}, u32[]{:S(2)}) copy-start(f32[2]{0:T(128)S(1)} %bitcast_convert_fusion.12) | copy-start | bytes 28
  73.3 52.0 %copy-start.3 = (f32[6,128,2,64]{1,0,3,2:T(8,128)S(1)}, f32[6,128,2,64]{1,0,3,2:T(8,128)}, u32[]{:S(2)}) copy-start(f32[6,128,2,64]{1,0,3,2:T(8,128)} %get-tuple-element.84) | copy-start | bytes 1179652
  87.2 0.9 copy-start.12
  87.2 1.1 copy-start.11
  87.2 23.5 %copy-start.10 = (f32[2]{0:T(128)}, f32[2]{0:T(128)S(1)}, u32[]{:S(2)}) copy-start(f32[2]{0:T(128)S(1)} %get-tuple-element.255) | copy-start | bytes 28
  139.0 1.1 copy-start.2
  142.8 5.0 %copy-start.13 = (bf16[2048]{0:T(1024)(128)(2,1)S(1)}, bf16[2048]{0:T(1024)(128)(2,1)}, u32[]{:S(2)}) copy-start(bf16[2048]{0:T(1024)(128)(2,1)} %param.33) | copy-start | bytes 12292
  142.8 33.0 %all-to-all-start = ((bf16[4,192,2048]{2,1,0:T(8,128)(2,1)}), bf16[4,192,2048]{2,1,0:T(8,128)(2,1)}, u32[]{:S(2)}, u32[]{:S(2)}) async-start(bf16[4,192,2048]{2,1,0:T(8,128)(2,1)} %bitcast.454), calls=%async_computation | async-start | bytes 6291456 | tf_op jit(solution)/shard_map/all_to_all | solution.py:82
  147.6 30.9 %copy-start.1 = (bf16[192,2048]{1,0:T(8,128)(2,1)S(1)}, bf16[192,2048]{1,0:T(8,128)(2,1)}, u32[]{:S(2)}) copy-start(bf16[192,2048]{1,0:T(8,128)(2,1)} %param.20) | copy-start | bytes 2359300
  147.6 81.0 %all-gather.9.cloned.1.call-start = ((), (), s32[]{:S(2)}) async-start(), calls=%async_computation.2 | async-start | bytes 3932160 | tf_op jit(solution)/shard_map/all_gather | solution.py:223
  178.5 1.6 copy-start.7
  178.5 1.6 copy-start.8
  180.0 151.5 %all-gather.11.cloned.1.call-start = ((), (), s32[]{:S(2)}) async-start(), calls=%async_computation.3 | async-start | bytes 17039360 | tf_op jit(solution)/shard_map/all_gather | solution.py:20
  180.8 208.9 %reduce-scatter.2.cloned.1.call-start = ((), (), s32[]{:S(2)}) async-start(), calls=%async_computation.4 | async-start | bytes 3932160 | tf_op jit(solution)/shard_map/reduce_scatter | solution.py:227
Sparse Core Ops, SparseCore 0:
  180.1 48.4 all-gather.8
  231.4 100.0 all-gather.10
  352.4 37.3 reduce-scatter.1
where the time goes:
time: 400 us; the launch traced here: 399 us
  waiting for transfers between devices  216 us (54%)
  local copies, waits for them, and re-layouts  50.2 us (13%)
  matrix products  35.7 us (9%)
  blocking collectives  35.5 us (9%)
  between operations  26.9 us (7%)
  other arithmetic  24.5 us (6%)
  starting transfers between devices  5.08 us (1%)
  loops' own time  4.6 us (1%)
    all_gather x1, waiting for transfers between devices, rows_first(): out, at, finished = (lax.all_gather(both, axis, axis=0, tiled=True), 0, [])  103 us
    all_gather x1, waiting for transfers between devices, on_device(): lax.all_gather(row_norm(middle, norm_gain), 'tp', axis=0, tiled=True)  47.7 us
    reduce_scatter x1, waiting for transfers between devices, on_device(): lax.psum_scatter(down_sum.astype(jnp.bfloat16), 'tp', scatter_dimension=0...  37.5 us
    all_gather x3, blocking collectives, gathered_once(): both, at, found = (lax.all_gather(jnp.concatenate(lines), axis), 0, {})  35.5 us
    all_to_all x1, waiting for transfers between devices, sum_at_owner(): lax.all_to_all(tiles, axis, split_axis=0, concat_axis=0, tiled=True)  27.9 us
    dynamic_update_slice x18, local copies, waits for them, and re-layouts, local_group(): lax.scan(block_step, carried, (query_rot.reshape(blocks, BLOCK, count_of_...  21.1 us
    dot_general x1, matrix products, on_device(): down_sum = jnp.dot(hidden, down_full, preferred_element_type=jnp.float32)  20.7 us
    convert_element_type x28, local copies, waits for them, and re-layouts, entering(): part[k].astype(own.dtype)  12.1 us
  transfers between devices with their start and end apart: 4, of which 4 were waited for; matrix products, arithmetic and copies ran while one was open for 0% of the time, Pallas kernels for 0%

commit v1 on v0

--- a/solution.py
+++ b/solution.py
@@ -193,6 +193,21 @@
     up_weight,
     down_weight,
 ):
+
+    def press_digits(x0, peer_axis):
+        n_all = jax.lax.axis_size(peer_axis)
+        buffers = list(map(lambda num: (num, (num + 1) % n_all), range(n_all)))
+        nodes = list(map(lambda num: (num, (num - 1) % n_all), range(n_all)))
+        seen_now, e_next = ([x0], [x0])
+        for _ in range(n_all // 2):
+            block_last = jax.lax.ppermute(seen_now[-1], peer_axis, buffers)
+            seen_now.append(block_last)
+        for _ in range((n_all - 1) // 2):
+            value_now = jax.lax.ppermute(e_next[-1], peer_axis, nodes)
+            e_next.append(value_now)
+        oldest = jnp.concatenate([*seen_now[::-1], *e_next[1:]], axis=0)
+        return jnp.roll(oldest, (jax.lax.axis_index(peer_axis) - n_all // 2) * x0.shape[0], axis=0)
+
     length = query_wide.shape[0]
     up_full, down_full = rows_first((up_weight, down_weight), SP, (0, 1))
     places = (lax.axis_index(SP) * length + jnp.arange(length, dtype=jnp.int32)).astype(jnp.float32)
@@ -220,7 +235,7 @@
         0,
     )
     middle = (stream_in.astype(jnp.float32) + mixed_sum).astype(jnp.bfloat16)
-    normed = lax.all_gather(row_norm(middle, norm_gain), "tp", axis=0, tiled=True)
+    normed = press_digits(row_norm(middle, norm_gain), peer_axis="tp")
     up_sum = jnp.dot(normed, up_full, preferred_element_type=jnp.float32)
     hidden = jnp.square(jax.nn.relu(up_sum)).astype(jnp.bfloat16)
     down_sum = jnp.dot(hidden, down_full, preferred_element_type=jnp.float32)

time: 400 us -> 305 us (0.76)
  waiting for transfers between devices: 216 us -> 103 us
  local copies, waits for them, and re-layouts: 50.2 us -> 57.5 us
  blocking collectives: 35.5 us -> 40.2 us
    all_gather x1, waiting for transfers between devices: 103 us -> 0.01 us  [rows_first(): out, at, finished = (lax.all_gather(both, axis, axis=0, tiled=True), 0, [])]
    all_gather x1 -> x0, waiting for transfers between devices: 47.7 us -> none  [on_device(): lax.all_gather(row_norm(middle, norm_gain), 'tp', axis=0, tiled=True)]
    ppermute x0 -> x3, waiting for transfers between devices: none -> 26.2 us  [the longest x2 26.2 us: press_digits(): block_last = jax.lax.ppermute(seen_now[-1], peer_axis, buffers)]
    reduce_scatter x1, waiting for transfers between devices: 37.5 us -> 46.6 us  [on_device(): lax.psum_scatter(down_sum.astype(jnp.bfloat16), 'tp', scatter_dimension=0...]
    unnamed x44 -> x55, local copies, waits for them, and re-layouts: 2.67 us -> 8.31 us
    all_gather x3, blocking collectives: 35.5 us -> 40.2 us  [gathered_once(): both, at, found = (lax.all_gather(jnp.concatenate(lines), axis), 0, {})]
  transfers between devices with their start and end apart: 4 -> 6, of which waited for: 4 -> 4; matrix products, arithmetic and copies ran while one was open for 0% -> 31% of each run, Pallas kernels for 0% -> 0%
where the time goes in v1:
time: 305 us; the launch traced here: 304 us
  waiting for transfers between devices  103 us (34%)
  local copies, waits for them, and re-layouts  57.5 us (19%)
  blocking collectives  40.2 us (13%)
  matrix products  36.1 us (12%)
  other arithmetic  26.8 us (9%)
  between operations  26.8 us (9%)
  starting transfers between devices  8.05 us (3%)
  loops' own time  4.56 us (1%)
    reduce_scatter x1, waiting for transfers between devices, on_device(): lax.psum_scatter(down_sum.astype(jnp.bfloat16), 'tp', scatter_dimension=0...  46.6 us
    all_gather x3, blocking collectives, gathered_once(): both, at, found = (lax.all_gather(jnp.concatenate(lines), axis), 0, {})  40.2 us
    all_to_all x1, waiting for transfers between devices, sum_at_owner(): lax.all_to_all(tiles, axis, split_axis=0, concat_axis=0, tiled=True)  30.6 us
    ppermute x2, waiting for transfers between devices, press_digits(): block_last = jax.lax.ppermute(seen_now[-1], peer_axis, buffers)  26.2 us
    dynamic_update_slice x18, local copies, waits for them, and re-layouts, local_group(): lax.scan(block_step, carried, (query_rot.reshape(blocks, BLOCK, count_of_...  21.1 us
    dot_general x1, matrix products, on_device(): down_sum = jnp.dot(hidden, down_full, preferred_element_type=jnp.float32)  20.8 us
    convert_element_type x28, local copies, waits for them, and re-layouts, entering(): part[k].astype(own.dtype)  11 us
    unnamed x55, local copies, waits for them, and re-layouts  8.31 us
  transfers between devices with their start and end apart: 6, of which 4 were waited for; matrix products, arithmetic and copies ran while one was open for 31% of the time, Pallas kernels for 0%

profile of v1, /device:TPU:1, one launch (start us, length us, event | category | flops | bytes accessed | tf_op | source)
XLA Modules:
  0.0 303.5 jit_solution(12342446104388072661)
XLA Ops:
  6.5 1.8 pad_maximum_fusion.2
  8.4 1.1 copy.156
  9.5 1.1 copy.158
  12.1 25.0 %while.27 = (s32[]{:T(128)}, f32[2,64,64]{2,1,0:T(8,128)S(1)}, f32[6,128,2,64]{1,0,3,2:T(8,128)}, f32[6,128,2]{2,1,0:T(8,128)S(1)}, f32[6,128,2,64]{1,0,3,2:T(8,...) while((s32[]{:T(128)}, f32[2,64,64]{2,1,0:T(8,128)S(1)}, ...), condition=%wide.region_5.6_spmd.clone, body=%wide.region_3.5_spmd.clone.sunk | while | flops 12877827 | bytes 1099440 | solution.py:132
  13.3 2.8 dynamic_update_slice.14
  17.4 2.8 dynamic_update_slice.14
  21.6 2.8 dynamic_update_slice.14
  25.7 2.8 dynamic_update_slice.14
  29.9 2.8 dynamic_update_slice.14
  34.1 2.8 dynamic_update_slice.14
  37.2 1.0 reshape_reshape.22
  44.4 1.0 bitcast_convert_fusion
  45.4 1.9 fusion.90
  47.4 0.9 maximum_multiply_fusion.1
  48.3 22.9 %while.26 = (s32[]{:T(128)}, f32[1,128,128]{2,1,0:T(8,128)S(1)}, f32[6,128,1,128]{3,1,0,2:T(8,128)}, f32[6,128,1]{1,2,0:T(1,128)S(1)}, f32[6,128,1,128]{3,2,1,0:...) while((s32[]{:T(128)}, f32[1,128,128]{2,1,0:T(8,128)S(1)}, ...), condition=%wide.region_2.3_spmd.clone, body=%wide.region_0.2_spmd.clone.sunk | while | flops 17006596 | bytes 1515172 | solution.py:132
  50.7 0.6 constant_dynamic-update-slice_fusion.10
  54.5 0.6 constant_dynamic-update-slice_fusion.10
  58.3 0.6 constant_dynamic-update-slice_fusion.10
  62.1 0.6 constant_dynamic-update-slice_fusion.10
  66.0 0.6 constant_dynamic-update-slice_fusion.10
  69.8 0.6 constant_dynamic-update-slice_fusion.10
  71.2 0.7 maximum_bitcast_fusion
  71.9 4.7 %all-gather.3 = bf16[2,194,128]{2,1,0:T(8,128)(2,1)S(1)} all-gather(bf16[1,194,128]{2,1,0:T(8,128)(2,1)S(1)} %maximum_bitcast_fusion), channel_id=2, replica_groups=mesh['sp_0'=8,'sp_1'=4,'sp_2'=2,'tp'=4] {'sp_2'}, dimensions={0}, use_global_device_ids=true | all-gather | bytes 148992 | tf_op jit(solution)/shard_map/all_gather | solution.py:42
  79.5 11.7 %all-gather.4 = bf16[4,194,128]{2,1,0:T(8,128)(2,1)S(1)} all-gather(bf16[1,194,128]{2,1,0:T(8,128)(2,1)S(1)} %maximum_bitcast_fusion.1), channel_id=3, replica_groups=mesh['sp_0'=8,'sp_1'=4,'sp_2'=2,'tp'=4] {'sp_1'}, dimensions={0}, use_global_device_ids=true | all-gather | bytes 248320 | tf_op jit(solution)/shard_map/all_gather | solution.py:42
  96.7 23.8 %all-gather.5 = bf16[8,194,128]{2,1,0:T(8,128)(2,1)S(1)} all-gather(bf16[1,194,128]{2,1,0:T(8,128)(2,1)S(1)} %maximum_bitcast_fusion.2), channel_id=4, replica_groups=mesh['sp_0'=8,'sp_1'=4,'sp_2'=2,'tp'=4] {'sp_0'}, dimensions={0}, use_global_device_ids=true | all-gather | bytes 446976 | tf_op jit(solution)/shard_map/all_gather | solution.py:42
  120.6 0.7 copy.173
  121.4 0.7 copy.174
  122.2 0.7 copy.175
  123.0 0.7 copy.176
  123.8 0.7 copy.177
  124.5 0.7 copy.178
  125.3 0.7 copy.179
  126.1 0.7 copy.180
  127.0 0.7 copy.181
  127.8 0.7 copy.182
  128.5 0.7 copy.183
  129.3 0.7 copy.184
  130.1 0.7 copy.185
  130.9 0.7 copy.186
  131.7 1.1 copy.170
  139.2 1.9 copy.169
  141.1 1.1 copy.153
  142.8 0.7 fusion.271
  143.5 1.5 fusion.295
  145.1 1.6 fusion.296
  147.0 1.0 fusion.95
  148.1 2.7 add_convert_fusion
  150.8 4.8 %all-to-all-start = ((bf16[4,192,2048]{2,1,0:T(8,128)(2,1)}), bf16[4,192,2048]{2,1,0:T(8,128)(2,1)}, u32[]{:S(2)}, u32[]{:S(2)}) async-start(bf16[4,192,2048]{2,1,0:T(8,128)(2,1)} %bitcast.453), calls=%async_computation | async-start | bytes 6291456 | tf_op jit(solution)/shard_map/all_to_all | solution.py:82
  155.8 30.6 %all-to-all-done = bf16[4,192,2048]{2,1,0:T(8,128)(2,1)} async-done(((bf16[4,192,2048]{2,1,0:T(8,128)(2,1)}), bf16[4,192,2048]{2,1,0:T(8,128)(2,1)}, u32[]{:S(2)}, u32[]{:S(2)}) %all-to-all-start) | async-done | bytes 3145760 | tf_op jit(solution)/shard_map/all_to_all | solution.py:82
  186.4 2.7 convert_reduce_fusion
  190.1 11.9 %collective-permute-done = bf16[192,2048]{1,0:T(8,128)(2,1)S(1)} collective-permute-done((bf16[192,2048]{1,0:T(8,128)(2,1)S(1)}, bf16[192,2048]{1,0:T(8,128)(2,1)S(1)}, u32[]{:S(2)}, u32[]{:S(2)}) %collective-permute-start) | collective-permute-done | bytes 786464 | tf_op jit(solution)/shard_map/ppermute | solution.py:203
  202.1 2.7 collective-permute-start.2
  204.8 14.2 %collective-permute-done.1 = bf16[192,2048]{1,0:T(8,128)(2,1)S(1)} collective-permute-done((bf16[192,2048]{1,0:T(8,128)(2,1)S(1)}, bf16[192,2048]{1,0:T(8,128)(2,1)S(1)}, u32[]{:S(2)}, u32[]{:S(2)}) %collective-permute-start.1) | collective-permute-done | bytes 786464 | tf_op jit(solution)/shard_map/ppermute | solution.py:203
  219.0 0.9 constant_dynamic-update-slice_fusion.8
  219.9 0.9 constant_dynamic-update-slice_fusion.7
  220.9 1.1 constant_dynamic-update-slice_fusion.6
  222.0 0.9 constant_dynamic-update-slice_fusion.5
  222.9 0.9 constant_dynamic-update-slice_fusion.4
  223.9 0.9 constant_dynamic-update-slice_fusion.3
  224.8 1.1 constant_dynamic-update-slice_fusion.2
  226.0 1.0 constant_dynamic-update-slice_fusion.1
  226.9 20.8 %fusion.55 = bf16[768,2048]{1,0:T(8,128)(2,1)} fusion(bf16[2048,4096]{1,0:T(8,128)(2,1)} %all-gather.8.cloned.1.call-done, bf16[1536,2048]{1,0:T(8,128)(2,1)} %constant_dynamic-update-slice_fusion.1, s32[]{:T(128)S(6)} %select_n.416), kind=kOutput, calls=%fused_computation.75 | convolution fusion | flops 12891193344 | bytes 23068676 | tf_op jit(solution)/shard_map/dot_general | solution.py:241
  247.8 46.6 %reduce-scatter.2.cloned.1.call-done = bf16[192,2048]{1,0:T(8,128)(2,1)} async-done(((bf16[768,2048]{1,0:T(8,128)(2,1)}), bf16[192,2048]{1,0:T(8,128)(2,1)}) %reduce-scatter.2.cloned.1.call-update) | async-done | bytes 786448 | tf_op jit(solution)/shard_map/reduce_scatter | solution.py:242
  294.4 2.3 fusion.66
  (305 shorter events, 36.0 us)
Async XLA Ops:
  6.5 140.5 %copy-start = (bf16[128,2048]{1,0:T(8,128)(2,1)S(1)}, bf16[128,2048]{1,0:T(8,128)(2,1)}, u32[]{:S(2)}) copy-start(bf16[128,2048]{1,0:T(8,128)(2,1)} %param.31) | copy-start | bytes 1572868
  6.5 4.7 %copy-start.6 = (bf16[768,128]{1,0:T(8,128)(2,1)S(1)}, bf16[768,128]{1,0:T(8,128)(2,1)}, u32[]{:S(2)}) copy-start(bf16[768,128]{1,0:T(8,128)(2,1)} %param.28) | copy-start | bytes 589828
  6.5 5.3 %copy-start.7 = (f32[2,768]{1,0:T(2,128)S(1)}, f32[2,768]{1,0:T(2,128)}, u32[]{:S(2)}) copy-start(f32[2,768]{1,0:T(2,128)} %param.30) | copy-start | bytes 18436
  6.5 220.4 %all-gather.8.cloned.1.call-start = ((), (), s32[]{:S(2)}) async-start(), calls=%async_computation.2 | async-start | bytes 17039360 | tf_op jit(solution)/shard_map/all_gather | solution.py:20
  11.3 26.9 %copy-start.16 = (f32[1,768]{1,0:T(1,128)S(1)}, f32[1,768]{1,0:T(1,128)}, u32[]{:S(2)}) copy-start(f32[1,768]{1,0:T(1,128)} %param.25) | copy-start | bytes 9220
  11.5 32.9 %copy-start.5 = (bf16[768,128]{1,0:T(8,128)(2,1)S(1)}, bf16[768,128]{1,0:T(8,128)(2,1)}, u32[]{:S(2)}) copy-start(bf16[768,128]{1,0:T(8,128)(2,1)} %param.21) | copy-start | bytes 589828
  38.9 0.5 copy-start.18
  71.2 60.4 %copy-start.4 = (f32[6,128,2,64]{1,0,3,2:T(8,128)S(1)}, f32[6,128,2,64]{1,0,3,2:T(8,128)}, u32[]{:S(2)}) copy-start(f32[6,128,2,64]{1,0,3,2:T(8,128)} %get-tuple-element.84) | copy-start | bytes 1179652
  77.8 13.4 %copy-start.10 = (f32[2]{0:T(128)}, f32[2]{0:T(128)S(1)}, u32[]{:S(2)}) copy-start(f32[2]{0:T(128)S(1)} %get-tuple-element.262) | copy-start | bytes 28
  78.0 1.5 copy-start.17
  94.9 1.7 copy-start.8
  95.0 0.6 copy-start.14
  95.1 1.5 copy-start.12
  95.1 1.5 copy-start.13
  96.7 48.4 %copy-start.9 = (f32[2]{0:T(128)S(1)}, f32[2]{0:T(128)}, u32[]{:S(2)}) copy-start(f32[2]{0:T(128)} %copy-done.8) | copy-start | bytes 28
  126.9 18.2 %copy-start.11 = (f32[2]{0:T(128)S(1)}, f32[2]{0:T(128)}, u32[]{:S(2)}) copy-start(f32[2]{0:T(128)} %copy-done.10) | copy-start | bytes 28
  146.9 1.2 copy-start.3
  148.1 7.7 %copy-start.15 = (bf16[2048]{0:T(1024)(128)(2,1)S(1)}, bf16[2048]{0:T(1024)(128)(2,1)}, u32[]{:S(2)}) copy-start(bf16[2048]{0:T(1024)(128)(2,1)} %param.33) | copy-start | bytes 12292
  150.8 38.4 %copy-start.1 = (bf16[192,2048]{1,0:T(8,128)(2,1)S(1)}, bf16[192,2048]{1,0:T(8,128)(2,1)}, u32[]{:S(2)}) copy-start(bf16[192,2048]{1,0:T(8,128)(2,1)} %param.20) | copy-start | bytes 2359300
  150.8 35.7 %all-to-all-start = ((bf16[4,192,2048]{2,1,0:T(8,128)(2,1)}), bf16[4,192,2048]{2,1,0:T(8,128)(2,1)}, u32[]{:S(2)}, u32[]{:S(2)}) async-start(bf16[4,192,2048]{2,1,0:T(8,128)(2,1)} %bitcast.453), calls=%async_computation | async-start | bytes 6291456 | tf_op jit(solution)/shard_map/all_to_all | solution.py:82
  155.6 138.8 %reduce-scatter.2.cloned.1.call-start = ((), (), s32[]{:S(2)}) async-start(), calls=%async_computation.3 | async-start | bytes 3932160 | tf_op jit(solution)/shard_map/reduce_scatter | solution.py:242
  189.8 12.3 %copy-start.2 = (bf16[192,2048]{1,0:T(8,128)(2,1)}, bf16[192,2048]{1,0:T(8,128)(2,1)S(1)}, u32[]{:S(2)}) copy-start(bf16[192,2048]{1,0:T(8,128)(2,1)S(1)} %fusion.65) | copy-start | bytes 2359300
  189.8 12.3 %collective-permute-start = (bf16[192,2048]{1,0:T(8,128)(2,1)S(1)}, bf16[192,2048]{1,0:T(8,128)(2,1)S(1)}, u32[]{:S(2)}, u32[]{:S(2)}) collective-permute-start(bf16[192,2048]{1,0:T(8,128)(2,1)S(1)} %fusion.65), channel_id=1, source_target_pairs={{0,1},{1,2},{2,3},{3,0},{4,5},{5,6},{6,7},{7,4},{8,9},{9,10},{10,1... | collective-permute-start | bytes 2359304 | tf_op jit(solution)/shard_map/ppermute | solution.py:203
  202.1 16.9 %collective-permute-start.1 = (bf16[192,2048]{1,0:T(8,128)(2,1)S(1)}, bf16[192,2048]{1,0:T(8,128)(2,1)S(1)}, u32[]{:S(2)}, u32[]{:S(2)}) collective-permute-start(bf16[192,2048]{1,0:T(8,128)(2,1)S(1)} %collective-permute-done), channel_id=1, source_target_pairs={{0,1},{1,2},{2,3},{3,0},{4,5},{5,6},{6,7},{7,4},{8,9},{9,10},{10,1... | collective-permute-start | bytes 2359304 | tf_op jit(solution)/shard_map/ppermute | solution.py:203
  202.1 19.9 %collective-permute-start.2 = (bf16[192,2048]{1,0:T(8,128)(2,1)}, bf16[192,2048]{1,0:T(8,128)(2,1)S(1)}, u32[]{:S(2)}, u32[]{:S(2)}) collective-permute-start(bf16[192,2048]{1,0:T(8,128)(2,1)} %copy-done.2), channel_id=1, source_target_pairs={{0,3},{1,0},{2,1},{3,2},{4,7},{5,4},{6,5},{7,6},{8,11},{9,8},{10,9... | collective-permute-start | bytes 2359304 | tf_op jit(solution)/shard_map/ppermute | solution.py:206
Sparse Core Ops, SparseCore 0:
  10.1 106.7 all-gather.7
  247.9 46.4 reduce-scatter.1
